TPU v7x, 128 devices: a whole 4x4x4 slice. The times are simulated.
128 devices in a mesh: kv: 32 (over z, y, core), tp: 4 (over x).
Axes of the slice: x: 4, y: 4, z: 4, core: 2. Of those that a mesh axis runs over, the one named last changes fastest.
Arguments:
- tokens: bfloat16 [512, 4, 4096], P('kv'), may hold values from -6 to 6
- norm_gain: bfloat16 [4096], replicated, may hold values from 0.099609375 to 1.8984375
- query_weight: bfloat16 [4096, 2048], P(None, 'tp'), may hold values from -0.09375 to 0.09375
- key_weight: bfloat16 [4096, 2048], P(None, 'tp'), may hold values from -0.09375 to 0.09375
- value_weight: bfloat16 [4096, 2048], P(None, 'tp'), may hold values from -0.09375 to 0.09375
- outgate_weight: bfloat16 [4096, 2048], P(None, 'tp'), may hold values from -0.09375 to 0.09375
- gate_weight: bfloat16 [4096, 32], replicated, may hold values from -0.09375 to 0.09375
- gate_bias: float32 [2, 16], replicated, may hold values from -1 to 4
- head_gain: bfloat16 [2048], P('tp'), may hold values from 0.099609375 to 1.8984375
- out_weight: bfloat16 [2048, 4096], P('tp', 'kv'), may hold values from -0.125 to 0.125
- state_c: float32 [512, 16, 128, 128], P('kv', 'tp'), may hold values from -3 to 3
- state_n: float32 [512, 16, 128], P('kv', 'tp'), may hold values from -3 to 3
- state_m: float32 [512, 16], P('kv', 'tp'), may hold values from -1 to 2
- prev_keys: bfloat16 [512, 16, 4, 128], P('kv', 'tp'), may hold values from -6 to 6
- prev_values: bfloat16 [512, 16, 4, 128], P('kv', 'tp'), may hold values from -6 to 6
- prev_gates: float32 [512, 16, 2, 4], P('kv', 'tp'), may hold values from -2 to 5
- accepted: int32 [512], P('kv'), may hold values from 0 to 4
Outputs:
- mixed: bfloat16 [512, 4, 4096], P(None, None, 'kv')
- carried_c: float32 [512, 16, 128, 128], P('kv', 'tp')
- carried_n: float32 [512, 16, 128], P('kv', 'tp')
- carried_m: float32 [512, 16], P('kv', 'tp')
- step_keys: bfloat16 [512, 16, 4, 128], P('kv', 'tp')
- step_values: bfloat16 [512, 16, 4, 128], P('kv', 'tp')
- step_gates: float32 [512, 16, 2, 4], P('kv', 'tp')
Inputs may be any that keep to these rules, and one draw needn't show every extreme that they name: accepted counts proposals of the last step, from none to all 4.
All inputs are finite; a program needn't handle non-finite values.
Results may differ from a plain program's by a relative error of at most 0.0075.
The roundings to bfloat16 on the way count: a program that leaves them out, or rounds other values in their place, can miss the bound.
Values may be sent and summed in bfloat16 or wider, within the bound.
No kernel may reach another device: no remote copies, remote signals or barrier semaphores. Data moves between devices by JAX's collectives and lax.ppermute only.
A program may use at most 128 MiB of HBM per device.

v0:
```python
import jax
import jax.numpy as jnp
from jax import lax
from jax.sharding import PartitionSpec as P

EPSILON = 1e-06
HIGHEST = lax.Precision.HIGHEST


def joined_along(tiles, dim):
    tiles = jnp.moveaxis(tiles, 0, dim)
    lengths = tiles.shape
    return tiles.reshape(*lengths[:dim], lengths[dim] * lengths[dim + 1], *lengths[dim + 2 :])


def from_everyone(x, axis):
    peers = lax.axis_size(axis)
    return lax.all_to_all(jnp.broadcast_to(x[None], (peers, *x.shape)), axis, 0, 0, tiled=True)


def collect(x, axis, dim):
    return joined_along(from_everyone(x, axis), dim)


def replay(state_c, state_n, state_m, keys_in, values_in, gates_in, accepted):
    proposals = keys_in.shape[2]
    scaled = keys_in.astype(jnp.float32) * keys_in.shape[3] ** (-0.5)
    values_f = values_in.astype(jnp.float32)
    igates = gates_in[:, :, 0, :]
    forget = jax.nn.log_sigmoid(gates_in[:, :, 1, :])
    position = jnp.arange(proposals, dtype=jnp.int32)
    within = position[None, None, :] < accepted[:, None, None]
    masked = jnp.where(within, forget, 0.0)
    summed = jnp.sum(masked, axis=-1)
    log_weight = jnp.where(
        within, summed[..., None] - jnp.cumsum(masked, axis=-1) + igates, -jnp.inf
    )
    carried_m = jnp.maximum(summed + state_m, jnp.max(log_weight, axis=-1))
    shrink = jnp.exp(summed + state_m - carried_m)
    weights = jnp.exp(log_weight - carried_m[..., None])
    carried_c = shrink[..., None, None] * state_c + jnp.einsum(
        "bhs,bhsv,bhsd->bhvd", weights, values_f, scaled, precision=HIGHEST
    )
    carried_n = shrink[..., None] * state_n + jnp.einsum(
        "bhs,bhsd->bhd", weights, scaled, precision=HIGHEST
    )
    return (carried_c, carried_n, carried_m)


def cell_block(state_c, state_n, state_m, queries, scaled, values_f, igates, forget):
    proposals = queries.shape[2]
    cumul = jnp.cumsum(forget, axis=-1)
    causal = jnp.tril(jnp.ones((proposals, proposals), dtype=bool))
    log_decay = jnp.where(
        causal, cumul[..., :, None] - cumul[..., None, :] + igates[..., None, :], -jnp.inf
    )
    carried = cumul + state_m[..., None]
    stable = jnp.maximum(carried, jnp.max(log_decay, axis=-1))
    scores = jnp.einsum("bhtd,bhsd->bhts", queries, scaled, precision=HIGHEST) * jnp.exp(
        log_decay - stable[..., None]
    )
    weight_state = jnp.exp(carried - stable)
    numer = weight_state[..., None] * jnp.einsum(
        "bhvd,bhtd->bhtv", state_c, queries, precision=HIGHEST
    )
    numer = numer + jnp.einsum("bhts,bhsv->bhtv", scores, values_f, precision=HIGHEST)
    denom = weight_state * jnp.einsum(
        "bhd,bhtd->bht", state_n, queries, precision=HIGHEST
    ) + jnp.sum(scores, axis=-1)
    return numer / jnp.maximum(jnp.abs(denom), jnp.exp(-stable))[..., None]


def gate_heads(hidden, gain, outgate):
    heads_count = hidden.shape[1]
    head_size = hidden.shape[3]
    normed = hidden * lax.rsqrt(jnp.mean(hidden * hidden, axis=-1, keepdims=True) + EPSILON)
    normed = normed * gain.astype(jnp.float32).reshape(heads_count, head_size)[None, :, None, :]
    rows_out = jnp.transpose(normed, (0, 2, 1, 3)).reshape(outgate.shape)
    return (rows_out * jax.nn.sigmoid(outgate.astype(jnp.float32))).astype(jnp.bfloat16)


def per_device(
    tokens,
    norm_gain,
    query_weight,
    key_weight,
    value_weight,
    outgate_weight,
    gate_weight,
    gate_bias,
    head_gain,
    out_weight,
    state_c,
    state_n,
    state_m,
    prev_keys,
    prev_values,
    prev_gates,
    accepted,
):
    seqs_local, proposals, features = tokens.shape
    heads_local = state_m.shape[1]
    head_size = state_n.shape[2]
    tokens_f = tokens.astype(jnp.float32)
    normed = tokens_f * lax.rsqrt(jnp.mean(tokens_f * tokens_f, axis=-1, keepdims=True) + EPSILON)
    normed = (normed * norm_gain.astype(jnp.float32)).astype(jnp.bfloat16)
    rows_in = normed.reshape(seqs_local * proposals, features)

    def project(matrix):
        return jnp.dot(rows_in, matrix, preferred_element_type=jnp.float32).astype(jnp.bfloat16)

    def by_head(array):
        return array.reshape(seqs_local, proposals, heads_local, head_size).transpose(0, 2, 1, 3)

    queries = project(query_weight)
    keys_new = project(key_weight)
    values_new = project(value_weight)
    outgate = project(outgate_weight)
    all_gates = (
        jnp.dot(rows_in, gate_weight, preferred_element_type=jnp.float32)
        + gate_bias.reshape(-1)[None, :]
    )
    heads_total = gate_weight.shape[1] // 2
    head_offset = lax.axis_index("tp") * heads_local
    igates = lax.dynamic_slice_in_dim(all_gates, head_offset, heads_local, 1)
    fgates = lax.dynamic_slice_in_dim(all_gates, heads_total + head_offset, heads_local, 1)
    igates = igates.reshape(seqs_local, proposals, heads_local).transpose(0, 2, 1)
    fgates = fgates.reshape(seqs_local, proposals, heads_local).transpose(0, 2, 1)
    step_gates = jnp.stack([igates, fgates], axis=2)
    carried_c, carried_n, carried_m = replay(
        state_c, state_n, state_m, prev_keys, prev_values, prev_gates, accepted
    )
    step_keys = by_head(keys_new)
    step_values = by_head(values_new)
    hidden = cell_block(
        carried_c,
        carried_n,
        carried_m,
        by_head(queries).astype(jnp.float32),
        step_keys.astype(jnp.float32) * head_size ** (-0.5),
        step_values.astype(jnp.float32),
        igates,
        jax.nn.log_sigmoid(fgates),
    )
    gated = gate_heads(hidden, head_gain, outgate)
    partial_out = jnp.dot(collect(gated, "kv", 0), out_weight, preferred_element_type=jnp.float32)
    summed = lax.psum(partial_out, "tp")
    mixed = summed.astype(jnp.bfloat16).reshape(-1, proposals, summed.shape[1])
    return (mixed, carried_c, carried_n, carried_m, step_keys, step_values, step_gates)


def solution(mesh):
    in_specs = (
        P("kv", None, None),
        P(),
        P(None, "tp"),
        P(None, "tp"),
        P(None, "tp"),
        P(None, "tp"),
        P(),
        P(),
        P("tp"),
        P("tp", "kv"),
        P("kv", "tp", None, None),
        P("kv", "tp", None),
        P("kv", "tp"),
        P("kv", "tp", None, None),
        P("kv", "tp", None, None),
        P("kv", "tp", None, None),
        P("kv"),
    )
    out_specs = (
        P(None, None, "kv"),
        P("kv", "tp", None, None),
        P("kv", "tp", None),
        P("kv", "tp"),
        P("kv", "tp", None, None),
        P("kv", "tp", None, None),
        P("kv", "tp", None, None),
    )
    return jax.shard_map(
        per_device, mesh=mesh, in_specs=in_specs, out_specs=out_specs, check_vma=False
    )
```

profile of v0, /device:TPU:0, one launch (start us, length us, event | category | flops | bytes accessed | tf_op | source)
XLA Modules:
  0.0 114.7 jit_solution(9230726068473415681)
XLA Ops:
  0.7 0.8 add.110
  1.5 0.7 iota_compare_fusion
  2.2 0.7 bitcast_convert_fusion
  2.9 0.8 copy.77
  3.6 1.4 %fusion.7 = f32[16,4]{1,0:T(8,128)S(1)} fusion(bf16[16,4,4096]{2,1,0:T(4,128)(2,1)} %param.17), kind=kLoop, calls=%fused_computation.16 | loop fusion | flops 786368 | bytes 524544 | tf_op jit(solution)/shard_map/reduce_sum | solution.py:105
  5.0 0.7 convert_element_type.41
  5.7 0.7 fusion.41
  6.7 1.4 %fusion.9 = bf16[16,4,4096]{2,1,0:T(4,128)(2,1)S(1)} fusion(bf16[16,4,4096]{2,1,0:T(4,128)(2,1)} %param.17, f32[4096]{0:T(1024)S(1)} %convert_element_type.41, f32[16,4]{1,0:T(8,128)S(1)} %add_rsqrt_fusion), kind=kLoop, calls=%fused_computation.18 | loop fusion | flops 1048576 | bytes 1065216 | tf_op jit(solution)/shard_map/convert_element_type | solution.py:106
  8.9 2.8 %reduce_window_sum.18 = f32[16,4,4]{2,1,0:T(4,128)S(1)} reduce-window(f32[16,4,4]{2,1,0:T(4,128)S(1)} %get-tuple-element.26, f32[]{:T(128)} %constant.13.clone.1), window={size=1x1x4 pad=0_0x0_0x3_0}, to_apply=%region_3.4 | reduce-window | flops 768 | bytes 2052 | tf_op jit(solution)/shard_map/jit(cumsum)/reduce_window_sum | solution.py:36
  11.7 2.7 %reduce_window_sum.17 = f32[16,4,4]{2,1,0:T(4,128)S(1)} reduce-window(f32[16,4,4]{2,1,0:T(4,128)S(1)} %fusion.24, f32[]{:T(128)} %constant.13.clone.1), window={size=1x1x4 pad=0_0x0_0x3_0}, to_apply=%region_1.2 | reduce-window | flops 768 | bytes 2052 | tf_op jit(solution)/shard_map/jit(cumsum)/reduce_window_sum | solution.py:52
  14.4 3.0 %convolution_convert_fusion.1 = bf16[64,512]{1,0:T(8,128)(2,1)S(1)} fusion(bf16[64,4096]{1,0:T(8,128)(2,1)S(1)} %reshape.103, bf16[4096,512]{1,0:T(8,128)(2,1)} %param.21), kind=kOutput, calls=%fused_computation.12 | convolution fusion | flops 268468224 | bytes 4784128 | tf_op jit(solution)/shard_map/dot_general | solution.py:110
  17.5 3.1 %convolution_convert_fusion.2 = bf16[64,512]{1,0:T(8,128)(2,1)S(1)} fusion(bf16[64,4096]{1,0:T(8,128)(2,1)S(1)} %reshape.103, bf16[4096,512]{1,0:T(8,128)(2,1)} %param.20), kind=kOutput, calls=%fused_computation.13 | convolution fusion | flops 268468224 | bytes 4784128 | tf_op jit(solution)/shard_map/dot_general | solution.py:110
  20.6 3.1 %convolution_convert_fusion.3 = bf16[64,512]{1,0:T(8,128)(2,1)S(1)} fusion(bf16[64,4096]{1,0:T(8,128)(2,1)S(1)} %reshape.103, bf16[4096,512]{1,0:T(8,128)(2,1)} %param.19), kind=kOutput, calls=%fused_computation.14 | convolution fusion | flops 268468224 | bytes 4784128 | tf_op jit(solution)/shard_map/dot_general | solution.py:110
  26.0 9.1 %multiply_add_fusion = f32[16,4,128,128]{3,2,1,0:T(8,128)S(1)} fusion(f32[16,4,128,128]{3,2,1,0:T(8,128)} %param.27, f32[16,4]{1,0:T(8,128)S(1)} %get-tuple-element.23, bf16[16,4,4,128]{3,2,1,0:T(4,128)(2,1)S(1)} %copy-done.4, bf16[16,4,4,128]{3,2,1,0:T(4,128)(2,1)S(1)} %copy-done.5, f32[16,4,4]{2,1,0:T(4,128)S(1)} %get-tuple-element.33), kind=kOutput, calls=%fused_computation | convolution fusion | flops 52559872 | bytes 8520960 | tf_op jit(solution)/shard_map/bhs,bhsv,bhsd->bhvd/dot_general | solution.py:41
  35.2 3.3 %fusion.23 = f32[16,4,4,128]{3,2,1,0:T(4,128)S(1)} fusion(f32[16,4,128,128]{3,2,1,0:T(8,128)S(1)} %multiply_add_fusion, bf16[16,4,4,128]{3,2,1,0:T(4,128)(2,1)S(1)} %reshape.106), kind=kOutput, calls=%fused_computation.43 | convolution fusion | flops 50331648 | bytes 4390912 | tf_op jit(solution)/shard_map/bhvd,bhtd->bhtv/dot_general | solution.py:63
  38.5 0.6 fusion.17
  39.5 0.9 fusion.6
  40.4 1.6 %broadcast_in_dim.52 = bf16[32,64,512]{2,1,0:T(8,128)(2,1)} broadcast(bf16[64,512]{1,0:T(8,128)(2,1)S(1)} %fusion.6), dimensions={1,2} | broadcast | bytes 2162688 | tf_op jit(solution)/shard_map/broadcast_in_dim | solution.py:18
  42.0 8.4 %all-to-all-start = ((bf16[32,64,512]{2,1,0:T(8,128)(2,1)}), bf16[32,64,512]{2,1,0:T(8,128)(2,1)S(1)}, u32[]{:S(2)}, u32[]{:S(2)}) async-start(bf16[32,64,512]{2,1,0:T(8,128)(2,1)} %broadcast_in_dim.52), calls=%async_computation | async-start | bytes 4194304 | tf_op jit(solution)/shard_map/all_to_all | solution.py:18
  50.4 0.7 copy.87
  51.3 0.6 pad_maximum_fusion
  51.9 28.6 %all-to-all-done = bf16[32,64,512]{2,1,0:T(8,128)(2,1)S(1)} async-done(((bf16[32,64,512]{2,1,0:T(8,128)(2,1)}), bf16[32,64,512]{2,1,0:T(8,128)(2,1)S(1)}, u32[]{:S(2)}, u32[]{:S(2)}) %all-to-all-start) | async-done | bytes 2097184 | tf_op jit(solution)/shard_map/all_to_all | solution.py:18
  80.5 0.7 fusion.43
  81.2 33.5 %all-reduce.1 = bf16[2048,128]{1,0:T(8,128)(2,1)} all-reduce(f32[2048,128]{1,0:T(8,128)S(1)} %fusion.43), channel_id=1, replica_groups=mesh['kv'=32,'tp'=4] {'tp'}, use_global_device_ids=true, to_apply=%region_8.9 | all-reduce | flops 262144 | bytes 1572864 | tf_op jit(solution)/shard_map/psum | solution.py:147
  (52 shorter events, 3.9 us)
Async XLA Ops:
  0.6 7.6 %copy-start = (bf16[4096,32]{0,1:T(8,128)(2,1)S(1)}, bf16[4096,32]{0,1:T(8,128)(2,1)}, u32[]{:S(2)}) copy-start(bf16[4096,32]{0,1:T(8,128)(2,1)} %param.23) | copy-start | bytes 786436
  17.5 6.7 %copy-start.4 = (bf16[16,4,4,128]{3,2,1,0:T(4,128)(2,1)S(1)}, bf16[16,4,4,128]{3,2,1,0:T(4,128)(2,1)}, u32[]{:S(2)}) copy-start(bf16[16,4,4,128]{3,2,1,0:T(4,128)(2,1)} %param.30) | copy-start | bytes 196612
  20.6 4.3 %copy-start.8 = (f32[16,4,128]{2,1,0:T(4,128)S(1)}, f32[16,4,128]{2,1,0:T(4,128)}, u32[]{:S(2)}) copy-start(f32[16,4,128]{2,1,0:T(4,128)} %param.28) | copy-start | bytes 98308
  20.6 5.4 %copy-start.5 = (bf16[16,4,4,128]{3,2,1,0:T(4,128)(2,1)S(1)}, bf16[16,4,4,128]{3,2,1,0:T(4,128)(2,1)}, u32[]{:S(2)}) copy-start(bf16[16,4,4,128]{3,2,1,0:T(4,128)(2,1)} %param.31) | copy-start | bytes 196612
  24.9 10.3 %copy-start.7 = (bf16[16,4,4,128]{3,2,1,0:T(4,128)(2,1)}, bf16[16,4,4,128]{3,2,1,0:T(4,128)(2,1)S(1)}, u32[]{:S(2)}) copy-start(bf16[16,4,4,128]{3,2,1,0:T(4,128)(2,1)S(1)} %get-tuple-element.40) | copy-start | bytes 196612
  24.9 13.7 %copy-start.6 = (bf16[16,4,4,128]{3,2,1,0:T(4,128)(2,1)}, bf16[16,4,4,128]{3,2,1,0:T(4,128)(2,1)S(1)}, u32[]{:S(2)}) copy-start(bf16[16,4,4,128]{3,2,1,0:T(4,128)(2,1)S(1)} %get-tuple-element.39) | copy-start | bytes 196612
  25.0 0.8 copy-start.9
  35.2 5.2 %copy-start.1 = (f32[16,4,128,128]{3,2,1,0:T(8,128)}, f32[16,4,128,128]{3,2,1,0:T(8,128)S(1)}, u32[]{:S(2)}) copy-start(f32[16,4,128,128]{3,2,1,0:T(8,128)S(1)} %multiply_add_fusion) | copy-start | bytes 12582916
  35.2 4.3 %copy-start.2 = (bf16[4096,512]{1,0:T(8,128)(2,1)S(1)}, bf16[4096,512]{1,0:T(8,128)(2,1)}, u32[]{:S(2)}) copy-start(bf16[4096,512]{1,0:T(8,128)(2,1)} %param.22) | copy-start | bytes 12582916
  40.4 40.1 %copy-start.3 = (bf16[512,128]{1,0:T(8,128)(2,1)S(1)}, bf16[512,128]{1,0:T(8,128)(2,1)}, u32[]{:S(2)}) copy-start(bf16[512,128]{1,0:T(8,128)(2,1)} %param.26) | copy-start | bytes 393220
  42.0 38.5 %all-to-all-start = ((bf16[32,64,512]{2,1,0:T(8,128)(2,1)}), bf16[32,64,512]{2,1,0:T(8,128)(2,1)S(1)}, u32[]{:S(2)}, u32[]{:S(2)}) async-start(bf16[32,64,512]{2,1,0:T(8,128)(2,1)} %broadcast_in_dim.52), calls=%async_computation | async-start | bytes 4194304 | tf_op jit(solution)/shard_map/all_to_all | solution.py:18
where the time goes:
time: 115 us
  blocking collectives  33.5 us (29%)
  waiting for transfers between devices  28.6 us (25%)
  matrix products  25.4 us (22%)
  other arithmetic  12.3 us (11%)
  starting transfers between devices  8.44 us (7%)
  local copies, waits for them, and re-layouts  5.47 us (5%)
    psum x1, blocking collectives, per_device(): summed = lax.psum(partial_out, 'tp')  33.5 us
    all_to_all x1, waiting for transfers between devices, from_everyone(): lax.all_to_all(jnp.broadcast_to(x[None], (peers, *x.shape)), axis, 0, 0,...  28.6 us
    dot_general x4, matrix products, project(): jnp.dot(rows_in, matrix, preferred_element_type=jnp.float32)  9.99 us
    dot_general x1, matrix products, replay(): jnp.einsum('bhs,bhsv,bhsd->bhvd', weights, values_f, scaled, precision=HI...  9.09 us
    all_to_all x1, starting transfers between devices, from_everyone(): lax.all_to_all(jnp.broadcast_to(x[None], (peers, *x.shape)), axis, 0, 0,...  8.44 us
    dot_general x1, matrix products, cell_block(): jnp.einsum('bhvd,bhtd->bhtv', state_c, queries, precision=HIGHEST)  3.35 us
    another operation x1, other arithmetic, replay(): jnp.cumsum(masked, axis=-1)  2.76 us
    another operation x1, other arithmetic, cell_block(): cumul = jnp.cumsum(forget, axis=-1)  2.75 us
  transfers between devices with their start and end apart: 1, of which 1 were waited for; matrix products, arithmetic and copies ran while one was open for 1% of the time, Pallas kernels for 0%

commit v1 on v0

--- a/solution.py
+++ b/solution.py
@@ -144,7 +144,7 @@
     )
     gated = gate_heads(hidden, head_gain, outgate)
     partial_out = jnp.dot(collect(gated, "kv", 0), out_weight, preferred_element_type=jnp.float32)
-    summed = lax.psum(partial_out, "tp")
+    summed = jnp.sum(lax.all_gather(partial_out, "tp"), axis=0)
     mixed = summed.astype(jnp.bfloat16).reshape(-1, proposals, summed.shape[1])
     return (mixed, carried_c, carried_n, carried_m, step_keys, step_values, step_gates)
 

time: 115 us -> 143 us (1.24)
  waiting for transfers between devices: 28.6 us -> 44.6 us
  between operations: 1.02 us -> 14.4 us
  starting transfers between devices: 8.44 us -> 0.04 us
  other arithmetic: 12.3 us -> 15.7 us
  blocking collectives: 33.5 us -> 36.7 us
    all_gather x0 -> x1, waiting for transfers between devices: none -> 44.6 us  [per_device(): summed = jnp.sum(lax.all_gather(partial_out, 'tp'), axis=0)]
    all_to_all x0 -> x1, blocking collectives: none -> 36.7 us  [from_everyone(): lax.all_to_all(jnp.broadcast_to(x[None], (peers, *x.shape)), axis, 0, 0,...]
    psum x1 -> x0, blocking collectives: 33.5 us -> none  [per_device(): summed = lax.psum(partial_out, 'tp')]
    all_to_all x1 -> x0, waiting for transfers between devices: 28.6 us -> none  [from_everyone(): lax.all_to_all(jnp.broadcast_to(x[None], (peers, *x.shape)), axis, 0, 0,...]
    all_to_all x1 -> x0, starting transfers between devices: 8.44 us -> none  [from_everyone(): lax.all_to_all(jnp.broadcast_to(x[None], (peers, *x.shape)), axis, 0, 0,...]
    reduce_sum x0 -> x1, other arithmetic: none -> 3.37 us  [per_device(): summed = jnp.sum(lax.all_gather(partial_out, 'tp'), axis=0)]
where the time goes in v1:
time: 143 us; the launch traced here: 142 us
  waiting for transfers between devices  44.6 us (31%)
  blocking collectives  36.7 us (26%)
  matrix products  26.3 us (18%)
  other arithmetic  15.7 us (11%)
  between operations  14.4 us (10%)
  local copies, waits for them, and re-layouts  4.08 us (3%)
    all_gather x1, waiting for transfers between devices, per_device(): summed = jnp.sum(lax.all_gather(partial_out, 'tp'), axis=0)  44.6 us
    all_to_all x1, blocking collectives, from_everyone(): lax.all_to_all(jnp.broadcast_to(x[None], (peers, *x.shape)), axis, 0, 0,...  36.7 us
    dot_general x4, matrix products, project(): jnp.dot(rows_in, matrix, preferred_element_type=jnp.float32)  9.99 us
    dot_general x1, matrix products, replay(): jnp.einsum('bhs,bhsv,bhsd->bhvd', weights, values_f, scaled, precision=HI...  9.09 us
    reduce_sum x1, other arithmetic, per_device(): summed = jnp.sum(lax.all_gather(partial_out, 'tp'), axis=0)  3.37 us
    dot_general x1, matrix products, cell_block(): jnp.einsum('bhvd,bhtd->bhtv', state_c, queries, precision=HIGHEST)  3.35 us
  transfers between devices with their start and end apart: 1, of which 1 were waited for; matrix products, arithmetic and copies ran while one was open for 1% of the time, Pallas kernels for 0%

profile of v1, /device:TPU:0, one launch (start us, length us, event | category | flops | bytes accessed | tf_op | source)
XLA Modules:
  0.0 141.8 jit_solution(6936359981136050106)
XLA Ops:
  7.2 0.8 add.108
  8.0 0.7 iota_compare_fusion
  8.7 0.7 bitcast_convert_fusion
  9.4 0.8 copy.77
  10.2 1.4 fusion.7
  11.6 0.7 convert_element_type.45
  12.3 0.7 fusion.41
  13.2 1.4 fusion.9
  15.5 2.8 %reduce_window_sum.18 = f32[16,4,4]{2,1,0:T(4,128)S(1)} reduce-window(f32[16,4,4]{2,1,0:T(4,128)S(1)} %get-tuple-element.26, f32[]{:T(128)} %constant.13.clone.1), window={size=1x1x4 pad=0_0x0_0x3_0}, to_apply=%region_3.4 | reduce-window | flops 768 | bytes 2052 | tf_op jit(solution)/shard_map/jit(cumsum)/reduce_window_sum | solution.py:36
  18.2 2.7 %reduce_window_sum.17 = f32[16,4,4]{2,1,0:T(4,128)S(1)} reduce-window(f32[16,4,4]{2,1,0:T(4,128)S(1)} %fusion.24, f32[]{:T(128)} %constant.13.clone.1), window={size=1x1x4 pad=0_0x0_0x3_0}, to_apply=%region_1.2 | reduce-window | flops 768 | bytes 2052 | tf_op jit(solution)/shard_map/jit(cumsum)/reduce_window_sum | solution.py:52
  21.0 3.0 %convolution_convert_fusion.1 = bf16[64,512]{1,0:T(8,128)(2,1)S(1)} fusion(bf16[64,4096]{1,0:T(8,128)(2,1)S(1)} %reshape.103, bf16[4096,512]{1,0:T(8,128)(2,1)} %param.21), kind=kOutput, calls=%fused_computation.12 | convolution fusion | flops 268468224 | bytes 4784128 | tf_op jit(solution)/shard_map/dot_general | solution.py:110
  24.0 3.1 %convolution_convert_fusion.2 = bf16[64,512]{1,0:T(8,128)(2,1)S(1)} fusion(bf16[64,4096]{1,0:T(8,128)(2,1)S(1)} %reshape.103, bf16[4096,512]{1,0:T(8,128)(2,1)} %param.20), kind=kOutput, calls=%fused_computation.13 | convolution fusion | flops 268468224 | bytes 4784128 | tf_op jit(solution)/shard_map/dot_general | solution.py:110
  27.1 3.1 %convolution_convert_fusion.3 = bf16[64,512]{1,0:T(8,128)(2,1)S(1)} fusion(bf16[64,4096]{1,0:T(8,128)(2,1)S(1)} %reshape.103, bf16[4096,512]{1,0:T(8,128)(2,1)} %param.19), kind=kOutput, calls=%fused_computation.14 | convolution fusion | flops 268468224 | bytes 4784128 | tf_op jit(solution)/shard_map/dot_general | solution.py:110
  30.8 0.6 fusion.13
  32.6 9.1 %multiply_add_fusion = f32[16,4,128,128]{3,2,1,0:T(8,128)S(1)} fusion(f32[16,4,128,128]{3,2,1,0:T(8,128)} %param.27, f32[16,4]{1,0:T(8,128)S(1)} %get-tuple-element.23, bf16[16,4,4,128]{3,2,1,0:T(4,128)(2,1)S(1)} %copy-done.4, bf16[16,4,4,128]{3,2,1,0:T(4,128)(2,1)S(1)} %copy-done.5, f32[16,4,4]{2,1,0:T(4,128)S(1)} %get-tuple-element.33), kind=kOutput, calls=%fused_computation | convolution fusion | flops 52559872 | bytes 8520960 | tf_op jit(solution)/shard_map/bhs,bhsv,bhsd->bhvd/dot_general | solution.py:41
  41.7 3.3 %fusion.23 = f32[16,4,4,128]{3,2,1,0:T(4,128)S(1)} fusion(f32[16,4,128,128]{3,2,1,0:T(8,128)S(1)} %multiply_add_fusion, bf16[16,4,4,128]{3,2,1,0:T(4,128)(2,1)S(1)} %reshape.106), kind=kOutput, calls=%fused_computation.43 | convolution fusion | flops 50331648 | bytes 4390912 | tf_op jit(solution)/shard_map/bhvd,bhtd->bhtv/dot_general | solution.py:63
  45.1 0.6 fusion.17
  46.0 0.9 fusion.6
  47.2 36.7 %all_to_all.5 = bf16[32,64,512]{2,1,0:T(8,128)(2,1)S(1)} all-to-all(bf16[32,64,512]{2,1,0:T(8,128)(2,1)S(1)} %broadcast_in_dim.52), channel_id=1, replica_groups=mesh['kv'=32,'tp'=4] {'kv'}, dimensions={0} | all-to-all | bytes 4194304 | tf_op jit(solution)/shard_map/all_to_all | solution.py:18
  83.9 1.7 %fusion.43 = f32[2048,128]{1,0:T(8,128)} fusion(bf16[2048,512]{1,0:T(8,128)(2,1)S(1)} %bitcast.129, bf16[512,128]{1,0:T(8,128)(2,1)S(1)} %copy-done.3), kind=kOutput, calls=%fused_computation.84 | convolution fusion | flops 268435456 | bytes 3276800 | tf_op jit(solution)/shard_map/dot_general | solution.py:146
  85.6 0.7 copy.87
  86.4 0.6 pad_maximum_fusion
  87.1 44.6 %all-gather.3.cloned.1.call-done = f32[8192,128]{1,0:T(8,128)} async-done(((f32[2048,128]{1,0:T(8,128)}), f32[8192,128]{1,0:T(8,128)}) %all-gather.3.cloned.1.call-update) | async-done | bytes 4194320 | tf_op jit(solution)/shard_map/all_gather | solution.py:147
  131.6 3.4 %reduce_sum.52 = bf16[2048,128]{1,0:T(8,128)(2,1)} reduce(f32[4,2048,128]{2,1,0:T(8,128)} %bitcast.130, f32[]{:T(128)} %constant.13.clone.1), dimensions={0}, to_apply=%region_8.9 | reduce | flops 786432 | bytes 4718596 | tf_op jit(solution)/shard_map/reduce_sum | solution.py:147
  (54 shorter events, 3.6 us)
Async XLA Ops:
  7.2 7.6 %copy-start = (bf16[4096,32]{0,1:T(8,128)(2,1)S(1)}, bf16[4096,32]{0,1:T(8,128)(2,1)}, u32[]{:S(2)}) copy-start(bf16[4096,32]{0,1:T(8,128)(2,1)} %param.23) | copy-start | bytes 786436
  7.2 124.5 %all-gather.3.cloned.1.call-start = ((), (), s32[]{:S(2)}) async-start(), calls=%async_computation.1 | async-start | bytes 5242880 | tf_op jit(solution)/shard_map/all_gather | solution.py:147
  24.0 6.7 %copy-start.4 = (bf16[16,4,4,128]{3,2,1,0:T(4,128)(2,1)S(1)}, bf16[16,4,4,128]{3,2,1,0:T(4,128)(2,1)}, u32[]{:S(2)}) copy-start(bf16[16,4,4,128]{3,2,1,0:T(4,128)(2,1)} %param.30) | copy-start | bytes 196612
  27.1 4.3 %copy-start.8 = (f32[16,4,128]{2,1,0:T(4,128)S(1)}, f32[16,4,128]{2,1,0:T(4,128)}, u32[]{:S(2)}) copy-start(f32[16,4,128]{2,1,0:T(4,128)} %param.28) | copy-start | bytes 98308
  27.1 5.4 %copy-start.5 = (bf16[16,4,4,128]{3,2,1,0:T(4,128)(2,1)S(1)}, bf16[16,4,4,128]{3,2,1,0:T(4,128)(2,1)}, u32[]{:S(2)}) copy-start(bf16[16,4,4,128]{3,2,1,0:T(4,128)(2,1)} %param.31) | copy-start | bytes 196612
  31.4 10.3 %copy-start.7 = (bf16[16,4,4,128]{3,2,1,0:T(4,128)(2,1)}, bf16[16,4,4,128]{3,2,1,0:T(4,128)(2,1)S(1)}, u32[]{:S(2)}) copy-start(bf16[16,4,4,128]{3,2,1,0:T(4,128)(2,1)S(1)} %get-tuple-element.40) | copy-start | bytes 196612
  31.4 13.7 %copy-start.6 = (bf16[16,4,4,128]{3,2,1,0:T(4,128)(2,1)}, bf16[16,4,4,128]{3,2,1,0:T(4,128)(2,1)S(1)}, u32[]{:S(2)}) copy-start(bf16[16,4,4,128]{3,2,1,0:T(4,128)(2,1)S(1)} %get-tuple-element.39) | copy-start | bytes 196612
  31.5 10.2 %copy-start.9 = (f32[16,4,128]{2,1,0:T(4,128)}, f32[16,4,128]{2,1,0:T(4,128)S(1)}, u32[]{:S(2)}) copy-start(f32[16,4,128]{2,1,0:T(4,128)S(1)} %multiply_add_fusion.1) | copy-start | bytes 98308
  41.7 5.2 %copy-start.1 = (f32[16,4,128,128]{3,2,1,0:T(8,128)}, f32[16,4,128,128]{3,2,1,0:T(8,128)S(1)}, u32[]{:S(2)}) copy-start(f32[16,4,128,128]{3,2,1,0:T(8,128)S(1)} %multiply_add_fusion) | copy-start | bytes 12582916
  41.7 4.3 %copy-start.2 = (bf16[4096,512]{1,0:T(8,128)(2,1)S(1)}, bf16[4096,512]{1,0:T(8,128)(2,1)}, u32[]{:S(2)}) copy-start(bf16[4096,512]{1,0:T(8,128)(2,1)} %param.22) | copy-start | bytes 12582916
  46.9 36.9 %copy-start.3 = (bf16[512,128]{1,0:T(8,128)(2,1)S(1)}, bf16[512,128]{1,0:T(8,128)(2,1)}, u32[]{:S(2)}) copy-start(bf16[512,128]{1,0:T(8,128)(2,1)} %param.26) | copy-start | bytes 393220
Sparse Core Ops, SparseCore 0:
  85.7 45.8 all-gather.2
